TPU v7x, 256 devices: a 4x2x16 block of a 4x16x16 slice. The times are simulated.
256 devices in a mesh: grp: 2 (over y), ra: 16 (over z), cb: 8 (over x, core).
Axes of the slice: x: 4, y: 2, z: 16, core: 2. Of those that a mesh axis runs over, the one named last changes fastest.
The devices are a block of a 4x16x16 slice.
Arguments:
- tokens: bfloat16 [256, 2048], P('grp', 'ra'), parts along dimension 0, may hold values from -8 to 8
- first_gain: bfloat16 [2048], P('ra'), may hold values from 0.099609375 to 1.8984375
- first_gate: bfloat16 [2048, 5632], P('ra', 'cb'), may hold values from -0.125 to 0.125
- first_up: bfloat16 [2048, 5632], P('ra', 'cb'), may hold values from -0.125 to 0.125
- first_down: bfloat16 [5632, 2048], P('cb', 'ra'), may hold values from -0.078125 to 0.078125
- second_gain: bfloat16 [2048], P('ra'), may hold values from 0.099609375 to 1.8984375
- second_gate: bfloat16 [2048, 5632], P('ra', 'cb'), may hold values from -0.125 to 0.125
- second_up: bfloat16 [2048, 5632], P('ra', 'cb'), may hold values from -0.125 to 0.125
- second_down: bfloat16 [5632, 2048], P('cb', 'ra'), may hold values from -0.078125 to 0.078125
Outputs:
- latent_out: bfloat16 [256, 2048], P('grp', 'ra'), parts along dimension 0
There are 2 independent parts, one for each index of `grp`. A program takes and returns all parts, laid end to end along the dimension named above; an argument that names none is the same for every part. Nothing has to cross between parts.
All inputs are finite; a program needn't handle non-finite values.
Results may differ from a plain program's by a relative error of at most 0.0088.
Values may be sent and summed in bfloat16 or wider, within the bound.
A program may use at most 64 MiB of HBM per device.

v0:
```python
import jax
import jax.numpy as jnp
from jax import lax
from jax.sharding import PartitionSpec as P


def cut_along(shard, dim, size):
    shape = shard.shape
    tiles = shard.reshape(*shape[:dim], size, shape[dim] // size, *shape[dim + 1 :])
    return jnp.moveaxis(tiles, dim, 0)


def summed_on_arrival(shard, axis, dim):
    size = lax.axis_size(axis)
    tiles = lax.all_to_all(cut_along(shard, dim, size), axis, 0, 0, tiled=True)
    return jnp.sum(tiles, axis=0)


def copy_for_each(shard, axis):
    copies = jnp.broadcast_to(shard, (lax.axis_size(axis), *shard.shape))
    return lax.all_to_all(copies, axis, split_axis=0, concat_axis=0, tiled=True)


def taken_together(shard, axis):
    return copy_for_each(shard, axis).sum(axis=0)


def laid_out(tiles, dim):
    tiles = jnp.moveaxis(tiles, 0, dim)
    shape = tiles.shape
    return tiles.reshape(*shape[:dim], shape[dim] * shape[dim + 1], *shape[dim + 2 :])


def gathered_copies(shard, axis, dim):
    return laid_out(copy_for_each(shard, axis), dim)


def sublayer(x, gain, w_gate, w_up, w_down):
    xf = x.astype(jnp.float32)
    width = x.shape[1] * lax.axis_size("ra")
    rows = x.shape[0]
    squares = jnp.sum(xf * xf, axis=1)
    normed = (xf * gain.astype(jnp.float32)).astype(jnp.bfloat16)
    dims = (((0,), (1,)), ((), ()))
    gate_rows = lax.dot_general(w_gate, normed, dims, preferred_element_type=jnp.float32)
    up_rows = lax.dot_general(w_up, normed, dims, preferred_element_type=jnp.float32)
    shares = summed_on_arrival(jnp.concatenate([gate_rows, up_rows], axis=1), "ra", 0)
    total_sq = taken_together(squares, "ra")
    scale = lax.rsqrt(total_sq / width + 1e-06)
    hidden_t = (
        jax.nn.silu(shares[:, :rows] * scale[None, :]) * (shares[:, rows:] * scale[None, :])
    ).astype(jnp.bfloat16)
    partial_value = lax.dot_general(
        gathered_copies(hidden_t, "ra", 0),
        w_down,
        (((0,), (0,)), ((), ())),
        preferred_element_type=jnp.float32,
    )
    branch = taken_together(partial_value, "cb")
    return (0.5 * xf + 0.5 * branch).astype(jnp.bfloat16)


def per_device(
    tokens,
    first_gain,
    first_gate,
    first_up,
    first_down,
    second_gain,
    second_gate,
    second_up,
    second_down,
):
    middle = sublayer(tokens, first_gain, first_gate, first_up, first_down)
    return sublayer(middle, second_gain, second_gate, second_up, second_down)


def solution(mesh):
    placed = (
        P("grp", "ra"),
        P("ra"),
        P("ra", "cb"),
        P("ra", "cb"),
        P("cb", "ra"),
        P("ra"),
        P("ra", "cb"),
        P("ra", "cb"),
        P("cb", "ra"),
    )
    return jax.shard_map(
        per_device, mesh=mesh, in_specs=placed, out_specs=P("grp", "ra"), check_vma=False
    )
```

profile of v0, /device:TPU:33, one launch (start us, length us, event | category | flops | bytes accessed | tf_op | source)
XLA Modules:
  0.0 218.6 jit_solution(15765565628771889623)
XLA Ops:
  0.0 0.0 copy-start
  0.0 0.0 copy-start.1
  0.0 0.9 fusion.1
  0.9 0.6 broadcast_in_dim.24
  1.6 0.0 copy-start.7
  1.6 24.6 %all-to-all-start.1 = ((f32[16,1,128]{2,1,0:T(1,128)}), f32[16,1,128]{2,1,0:T(1,128)S(1)}, u32[]{:S(2)}, u32[]{:S(2)}) async-start(f32[16,1,128]{2,1,0:T(1,128)} %broadcast_in_dim.24), calls=%async_computation.1 | async-start | bytes 16384 | tf_op jit(solution)/shard_map/all_to_all | solution.py:21
  26.2 0.0 copy-done.7
  26.2 0.0 copy-done
  26.2 0.0 copy-done.1
  26.3 0.0 copy-start.4
  26.3 0.2 convolution_bitcast_fusion.2
  26.5 0.7 copy-done.4
  27.2 0.2 convolution_bitcast_fusion.3
  27.4 0.9 reshape.32
  28.4 8.9 %all-to-all-done.1 = f32[16,1,128]{2,1,0:T(1,128)S(1)} async-done(((f32[16,1,128]{2,1,0:T(1,128)}), f32[16,1,128]{2,1,0:T(1,128)S(1)}, u32[]{:S(2)}, u32[]{:S(2)}) %all-to-all-start.1) | async-done | bytes 8224 | tf_op jit(solution)/shard_map/all_to_all | solution.py:21
  37.3 4.1 %all-to-all-start = ((f32[16,44,256]{2,1,0:T(8,128)}), f32[16,44,256]{2,1,0:T(8,128)S(1)}, u32[]{:S(2)}, u32[]{:S(2)}) async-start(f32[16,44,256]{2,1,0:T(8,128)} %reshape.32), calls=%async_computation | async-start | bytes 1572864 | tf_op jit(solution)/shard_map/all_to_all | solution.py:15
  41.4 33.2 %all-to-all-done = f32[16,44,256]{2,1,0:T(8,128)S(1)} async-done(((f32[16,44,256]{2,1,0:T(8,128)}), f32[16,44,256]{2,1,0:T(8,128)S(1)}, u32[]{:S(2)}, u32[]{:S(2)}) %all-to-all-start) | async-done | bytes 720928 | tf_op jit(solution)/shard_map/all_to_all | solution.py:15
  74.5 0.1 reduce_sum.72
  74.7 25.4 %all_to_all.42 = bf16[16,44,128]{2,1,0:T(8,128)(2,1)S(1)} all-to-all(bf16[16,44,128]{2,1,0:T(8,128)(2,1)S(1)} %broadcast_in_dim.25), channel_id=1, replica_groups=mesh['grp'=2,'ra'=16,'cb'=8] {'ra'}, dimensions={0} | all-to-all | bytes 360448 | tf_op jit(solution)/shard_map/all_to_all | solution.py:21
  100.0 0.0 copy-start.2
  100.0 0.9 copy-done.2
  100.9 0.2 fusion.17
  101.2 0.8 broadcast_in_dim.26
  102.0 0.0 copy-start.8
  102.0 9.6 %all-to-all-start.3 = ((f32[8,128,128]{2,1,0:T(8,128)}), f32[8,128,128]{2,1,0:T(8,128)S(1)}, u32[]{:S(2)}, u32[]{:S(2)}) async-start(f32[8,128,128]{2,1,0:T(8,128)} %broadcast_in_dim.26), calls=%async_computation.3 | async-start | bytes 1048576 | tf_op jit(solution)/shard_map/all_to_all | solution.py:21
  111.6 0.0 copy-done.8
  111.6 9.3 %all-to-all-done.3 = f32[8,128,128]{2,1,0:T(8,128)S(1)} async-done(((f32[8,128,128]{2,1,0:T(8,128)}), f32[8,128,128]{2,1,0:T(8,128)S(1)}, u32[]{:S(2)}, u32[]{:S(2)}) %all-to-all-start.3) | async-done | bytes 524320 | tf_op jit(solution)/shard_map/all_to_all | solution.py:21
  120.9 0.0 copy-start.5
  120.9 0.1 fusion.5
  121.1 0.6 broadcast_in_dim.27
  121.7 4.9 %all-to-all-start.5 = ((f32[16,1,128]{2,1,0:T(1,128)}), f32[16,1,128]{2,1,0:T(1,128)S(1)}, u32[]{:S(2)}, u32[]{:S(2)}) async-start(f32[16,1,128]{2,1,0:T(1,128)} %broadcast_in_dim.27), calls=%async_computation.5 | async-start | bytes 16384 | tf_op jit(solution)/shard_map/all_to_all | solution.py:21
  126.6 0.0 copy-done.5
  126.6 0.0 copy-start.6
  126.6 0.2 convolution_bitcast_fusion
  126.8 0.7 copy-done.6
  127.5 0.2 convolution_bitcast_fusion.1
  127.7 0.1 pad_maximum_fusion.1
  127.8 0.9 reshape.34
  128.7 8.9 %all-to-all-done.5 = f32[16,1,128]{2,1,0:T(1,128)S(1)} async-done(((f32[16,1,128]{2,1,0:T(1,128)}), f32[16,1,128]{2,1,0:T(1,128)S(1)}, u32[]{:S(2)}, u32[]{:S(2)}) %all-to-all-start.5) | async-done | bytes 8224 | tf_op jit(solution)/shard_map/all_to_all | solution.py:21
  137.6 4.1 %all-to-all-start.4 = ((f32[16,44,256]{2,1,0:T(8,128)}), f32[16,44,256]{2,1,0:T(8,128)S(1)}, u32[]{:S(2)}, u32[]{:S(2)}) async-start(f32[16,44,256]{2,1,0:T(8,128)} %reshape.34), calls=%async_computation.4 | async-start | bytes 1572864 | tf_op jit(solution)/shard_map/all_to_all | solution.py:15
  141.7 33.2 %all-to-all-done.4 = f32[16,44,256]{2,1,0:T(8,128)S(1)} async-done(((f32[16,44,256]{2,1,0:T(8,128)}), f32[16,44,256]{2,1,0:T(8,128)S(1)}, u32[]{:S(2)}, u32[]{:S(2)}) %all-to-all-start.4) | async-done | bytes 720928 | tf_op jit(solution)/shard_map/all_to_all | solution.py:15
  174.9 0.1 reduce_sum.76
  175.0 24.8 %all_to_all.43 = bf16[16,44,128]{2,1,0:T(8,128)(2,1)S(1)} all-to-all(bf16[16,44,128]{2,1,0:T(8,128)(2,1)S(1)} %broadcast_in_dim.28), channel_id=1, replica_groups=mesh['grp'=2,'ra'=16,'cb'=8] {'ra'}, dimensions={0} | all-to-all | bytes 360448 | tf_op jit(solution)/shard_map/all_to_all | solution.py:21
  199.8 0.0 copy-start.3
  199.9 0.9 copy-done.3
  200.8 0.2 fusion.18
  201.1 16.9 %all_to_all.44 = f32[8,128,128]{2,1,0:T(8,128)S(1)} all-to-all(f32[8,128,128]{2,1,0:T(8,128)S(1)} %broadcast_in_dim.29), channel_id=1, replica_groups=mesh['grp'=2,'ra'=16,'cb'=8] {'cb'}, dimensions={0} | all-to-all | bytes 1048576 | tf_op jit(solution)/shard_map/all_to_all | solution.py:21
  218.0 0.6 fusion.7
  (16 shorter events, 0.4 us)
Async XLA Ops:
  0.0 26.2 %copy-start = (bf16[128,704]{0,1:T(8,128)(2,1)S(1)}, bf16[128,704]{0,1:T(8,128)(2,1)}, u32[]{:S(2)}) copy-start(bf16[128,704]{0,1:T(8,128)(2,1)} %param.12) | copy-start | bytes 540676
  0.0 26.2 %copy-start.1 = (bf16[128,128]{1,0:T(8,128)(2,1)S(1)}, bf16[128,128]{1,0:T(8,128)(2,1)}, u32[]{:S(2)}) copy-start(bf16[128,128]{1,0:T(8,128)(2,1)} %param.9) | copy-start | bytes 98308
  1.6 24.7 %copy-start.7 = (bf16[128]{0:T(256)(128)(2,1)S(1)}, bf16[128]{0:T(256)(128)(2,1)}, u32[]{:S(2)}) copy-start(bf16[128]{0:T(256)(128)(2,1)} %param.10) | copy-start | bytes 772
  1.6 35.7 %all-to-all-start.1 = ((f32[16,1,128]{2,1,0:T(1,128)}), f32[16,1,128]{2,1,0:T(1,128)S(1)}, u32[]{:S(2)}, u32[]{:S(2)}) async-start(f32[16,1,128]{2,1,0:T(1,128)} %broadcast_in_dim.24), calls=%async_computation.1 | async-start | bytes 16384 | tf_op jit(solution)/shard_map/all_to_all | solution.py:21
  26.3 0.9 copy-start.4
  37.3 37.3 %all-to-all-start = ((f32[16,44,256]{2,1,0:T(8,128)}), f32[16,44,256]{2,1,0:T(8,128)S(1)}, u32[]{:S(2)}, u32[]{:S(2)}) async-start(f32[16,44,256]{2,1,0:T(8,128)} %reshape.32), calls=%async_computation | async-start | bytes 1572864 | tf_op jit(solution)/shard_map/all_to_all | solution.py:15
  100.0 0.9 copy-start.2
  102.0 9.6 %copy-start.8 = (bf16[128]{0:T(256)(128)(2,1)S(1)}, bf16[128]{0:T(256)(128)(2,1)}, u32[]{:S(2)}) copy-start(bf16[128]{0:T(256)(128)(2,1)} %param.14) | copy-start | bytes 772
  102.0 18.9 %all-to-all-start.3 = ((f32[8,128,128]{2,1,0:T(8,128)}), f32[8,128,128]{2,1,0:T(8,128)S(1)}, u32[]{:S(2)}, u32[]{:S(2)}) async-start(f32[8,128,128]{2,1,0:T(8,128)} %broadcast_in_dim.26), calls=%async_computation.3 | async-start | bytes 1048576 | tf_op jit(solution)/shard_map/all_to_all | solution.py:21
  120.9 5.7 %copy-start.5 = (bf16[128,704]{0,1:T(8,128)(2,1)S(1)}, bf16[128,704]{0,1:T(8,128)(2,1)}, u32[]{:S(2)}) copy-start(bf16[128,704]{0,1:T(8,128)(2,1)} %param.16) | copy-start | bytes 540676
  121.7 16.0 %all-to-all-start.5 = ((f32[16,1,128]{2,1,0:T(1,128)}), f32[16,1,128]{2,1,0:T(1,128)S(1)}, u32[]{:S(2)}, u32[]{:S(2)}) async-start(f32[16,1,128]{2,1,0:T(1,128)} %broadcast_in_dim.27), calls=%async_computation.5 | async-start | bytes 16384 | tf_op jit(solution)/shard_map/all_to_all | solution.py:21
  126.6 0.9 copy-start.6
  137.6 37.3 %all-to-all-start.4 = ((f32[16,44,256]{2,1,0:T(8,128)}), f32[16,44,256]{2,1,0:T(8,128)S(1)}, u32[]{:S(2)}, u32[]{:S(2)}) async-start(f32[16,44,256]{2,1,0:T(8,128)} %reshape.34), calls=%async_computation.4 | async-start | bytes 1572864 | tf_op jit(solution)/shard_map/all_to_all | solution.py:15
  199.8 0.9 copy-start.3
where the time goes:
time: 219 us
  waiting for transfers between devices  93.5 us (43%)
  blocking collectives  67 us (31%)
  starting transfers between devices  47.2 us (22%)
  local copies, waits for them, and re-layouts  7.32 us (3%)
    all_to_all x3, blocking collectives, copy_for_each(): return lax.all_to_all(copies, axis, split_axis=0, concat_axis=0, tiled=True)  67 us
    all_to_all x2, waiting for transfers between devices, summed_on_arrival(): tiles = lax.all_to_all(cut_along(shard, dim, size), axis, 0, 0, tiled=True)  66.4 us
    all_to_all x3, starting transfers between devices, copy_for_each(): return lax.all_to_all(copies, axis, split_axis=0, concat_axis=0, tiled=True)  39.1 us
    all_to_all x3, waiting for transfers between devices, copy_for_each(): return lax.all_to_all(copies, axis, split_axis=0, concat_axis=0, tiled=True)  27.1 us
    all_to_all x2, starting transfers between devices, summed_on_arrival(): tiles = lax.all_to_all(cut_along(shard, dim, size), axis, 0, 0, tiled=True)  8.11 us
  transfers between devices with their start and end apart: 5, of which 5 were waited for; matrix products, arithmetic and copies ran while one was open for 1% of the time, Pallas kernels for 0%

commit v1 on v0

v1 whole, which is shorter than its diff:
```python
import functools

import jax
import jax.numpy as jnp
from jax import lax
from jax.experimental import pallas as pl
from jax.experimental.pallas import tpu as pltpu
from jax.sharding import PartitionSpec as P

MESH = pl.DeviceIdType.MESH
LANES = 128
BF16 = jnp.bfloat16
F32 = jnp.float32


def far_first(n):
    return sorted(range(1, n), key=lambda o: -min(o, n - o))


def fused(n_ra, n_cb, tokens, gain1, gate1, up1, down1, gain2, gate2, up2, down2, out,
          x_v, gain_v, gate_v, up_v, down_v, x_f,
          rs_out, rs_in, ag_out, ag_in, ar_in,
          load_sem, rs_send, rs_recv, ag_send, ag_recv, ar_send, ar_recv):
    ra = lax.axis_index("ra")
    cb = lax.axis_index("cb")
    rows, cols = x_v.shape
    oct_rows = rows // n_ra
    units = gate_v.shape[2]
    half = rs_in.shape[3] // 2
    width = cols * n_ra

    loads = [pltpu.make_async_copy(tokens, x_v, load_sem.at[0])]
    for s, (gn, gt, up, dn) in enumerate(((gain1, gate1, up1, down1), (gain2, gate2, up2, down2))):
        loads += [
            pltpu.make_async_copy(gn, gain_v.at[s], load_sem.at[4 * s + 1]),
            pltpu.make_async_copy(gt, gate_v.at[s], load_sem.at[4 * s + 2]),
            pltpu.make_async_copy(up, up_v.at[s], load_sem.at[4 * s + 3]),
            pltpu.make_async_copy(dn, down_v.at[s], load_sem.at[4 * s + 4]),
        ]
    for c in loads:
        c.start()

    barrier = pltpu.get_barrier_semaphore()
    for o in far_first(n_ra):
        pl.semaphore_signal(barrier, 1, device_id={"ra": lax.rem(ra + o, n_ra)}, device_id_type=MESH)
    for o in range(1, n_cb):
        pl.semaphore_signal(barrier, 1, device_id={"cb": lax.rem(cb + o, n_cb)}, device_id_type=MESH)

    for s in range(2):
        if s == 0:
            loads[0].wait()
            xf = x_v[...].astype(F32)
        else:
            xf = x_f[...]
        for c in loads[4 * s + 1:4 * s + 4]:
            c.wait()
        sq = jnp.sum(xf * xf, axis=1, keepdims=True)
        hi = sq.astype(BF16).astype(F32)
        normed = (xf * gain_v[s].astype(F32)).astype(BF16)
        pad = half - units
        for w, at, extra in ((gate_v, 0, hi), (up_v, half, sq - hi)):
            part = jnp.dot(normed, w[s], preferred_element_type=F32)
            rs_out[:, :, at:at + units] = part.reshape(n_ra, oct_rows, units).astype(BF16)
            rs_out[:, :, at + units:at + half] = jnp.broadcast_to(
                extra.reshape(n_ra, oct_rows, 1), (n_ra, oct_rows, pad)).astype(BF16)
        if s == 0:
            pl.semaphore_wait(barrier, n_ra - 1 + n_cb - 1)
        sends = []
        for o in far_first(n_ra):
            to = lax.rem(ra + o, n_ra)
            c = pltpu.make_async_remote_copy(
                src_ref=rs_out.at[to], dst_ref=rs_in.at[s, o], send_sem=rs_send.at[o],
                recv_sem=rs_recv.at[s, o], device_id={"ra": to}, device_id_type=MESH)
            c.start()
            sends.append(c)
        total = rs_out[ra].astype(F32)
        for o in reversed(far_first(n_ra)):
            pltpu.make_async_remote_copy(
                src_ref=rs_out.at[0], dst_ref=rs_in.at[s, o], send_sem=rs_send.at[o],
                recv_sem=rs_recv.at[s, o], device_id={"ra": ra}, device_id_type=MESH).wait_recv()
            total = total + rs_in[s, o].astype(F32)
        sumsq = total[:, units:units + 1] + total[:, half + units:half + units + 1]
        scale = lax.rsqrt(sumsq / width + 1e-06)
        g = total[:, :units] * scale
        hidden = (g / (1.0 + jnp.exp(-g)) * (total[:, half:half + units] * scale)).astype(BF16)
        ag_out[s] = hidden
        ag_in[s, ra] = hidden
        ag = []
        for o in far_first(n_ra):
            to = lax.rem(ra + o, n_ra)
            c = pltpu.make_async_remote_copy(
                src_ref=ag_out.at[s], dst_ref=ag_in.at[s, ra], send_sem=ag_send.at[o],
                recv_sem=ag_recv.at[s, o], device_id={"ra": to}, device_id_type=MESH)
            c.start()
            ag.append(c)
        loads[4 * s + 4].wait()
        for o in reversed(far_first(n_ra)):
            pltpu.make_async_remote_copy(
                src_ref=ag_out.at[s], dst_ref=ag_in.at[s, lax.rem(ra + n_ra - o, n_ra)], send_sem=ag_send.at[o],
                recv_sem=ag_recv.at[s, o], device_id={"ra": ra}, device_id_type=MESH).wait_recv()
        h = ag_in[s].astype(F32).reshape(rows, units).astype(BF16)
        ar_in[s, cb] = jnp.dot(h, down_v[s], preferred_element_type=F32).astype(BF16)
        ar = []
        for o in far_first(n_cb):
            c = pltpu.make_async_remote_copy(
                src_ref=ar_in.at[s, cb], dst_ref=ar_in.at[s, cb], send_sem=ar_send.at[o],
                recv_sem=ar_recv.at[s, o], device_id={"cb": lax.rem(cb + o, n_cb)}, device_id_type=MESH)
            c.start()
            ar.append(c)
        for o in reversed(far_first(n_cb)):
            pltpu.make_async_remote_copy(
                src_ref=ar_in.at[s, cb], dst_ref=ar_in.at[s, lax.rem(cb + n_cb - o, n_cb)], send_sem=ar_send.at[o],
                recv_sem=ar_recv.at[s, o], device_id={"cb": cb}, device_id_type=MESH).wait_recv()
        branch = ar_in[s, 0].astype(F32)
        for c in range(1, n_cb):
            branch = branch + ar_in[s, c].astype(F32)
        result = (0.5 * xf + 0.5 * branch).astype(BF16)
        if s == 0:
            x_f[...] = result.astype(F32)
        else:
            out[...] = result
        for c in sends + ag + ar:
            c.wait_send()


def per_device(tokens, first_gain, first_gate, first_up, first_down,
               second_gain, second_gate, second_up, second_down):
    n_ra, n_cb = lax.axis_size("ra"), lax.axis_size("cb")
    rows, cols = tokens.shape
    units = first_gate.shape[1]
    half = -(-units // LANES) * LANES
    if half == units:
        half += LANES
    o_rows = rows // n_ra
    dma = pltpu.SemaphoreType.DMA
    any_spec = pl.BlockSpec(memory_space=pl.ANY)
    return pl.pallas_call(
        functools.partial(fused, n_ra, n_cb),
        out_shape=jax.ShapeDtypeStruct((rows, cols), BF16),
        in_specs=[any_spec] * 9,
        out_specs=pl.BlockSpec(memory_space=pltpu.VMEM),
        scratch_shapes=[
            pltpu.VMEM((rows, cols), BF16),
            pltpu.VMEM((2, 1, cols), BF16),
            pltpu.VMEM((2, cols, units), BF16),
            pltpu.VMEM((2, cols, units), BF16),
            pltpu.VMEM((2, units, cols), BF16),
            pltpu.VMEM((rows, cols), F32),
            pltpu.VMEM((n_ra, o_rows, 2 * half), BF16),
            pltpu.VMEM((2, n_ra, o_rows, 2 * half), BF16),
            pltpu.VMEM((2, o_rows, units), BF16),
            pltpu.VMEM((2, n_ra, o_rows, units), BF16),
            pltpu.VMEM((2, n_cb, rows, cols), BF16),
            dma((9,)),
            dma((n_ra,)), dma((2, n_ra)),
            dma((n_ra,)), dma((2, n_ra)),
            dma((n_cb,)), dma((2, n_cb)),
        ],
        compiler_params=pltpu.CompilerParams(collective_id=0, has_side_effects=True),
    )(tokens, first_gain.reshape(1, -1), first_gate, first_up, first_down,
      second_gain.reshape(1, -1), second_gate, second_up, second_down)


def solution(mesh):
    placed = (
        P("grp", "ra"),
        P("ra"), P("ra", "cb"), P("ra", "cb"), P("cb", "ra"),
        P("ra"), P("ra", "cb"), P("ra", "cb"), P("cb", "ra"),
    )
    return jax.shard_map(
        per_device, mesh=mesh, in_specs=placed, out_specs=P("grp", "ra"), check_vma=False
    )
```

time: 219 us -> 106 us (0.48)
  Pallas kernels: 0 us -> 100 us
  waiting for transfers between devices: 93.5 us -> 0 us
  blocking collectives: 67 us -> 0 us
  starting transfers between devices: 47.2 us -> 0 us
    pallas_call x0 -> x1, Pallas kernels: none -> 100 us  [per_device(): pl.pallas_call(functools.partial(fused, n_ra, n_cb), out_shape=jax.ShapeD...]
    all_to_all x5 -> x0, waiting for transfers between devices: 93.5 us -> none  [the longest x2 66.4 us: summed_on_arrival(): tiles = lax.all_to_all(cut_along(shard, dim, size), axis, 0, 0, tiled=True)]
    all_to_all x3 -> x0, blocking collectives: 67 us -> none  [copy_for_each(): return lax.all_to_all(copies, axis, split_axis=0, concat_axis=0, tiled=True)]
    all_to_all x5 -> x0, starting transfers between devices: 47.2 us -> none  [the longest x3 39.1 us: copy_for_each(): return lax.all_to_all(copies, axis, split_axis=0, concat_axis=0, tiled=True)]
    unnamed x18 -> x11, local copies, waits for them, and re-layouts: 3.2 us -> 5.8 us
  transfers between devices with their start and end apart: 5 -> 0, of which waited for: 5 -> 0; matrix products, arithmetic and copies ran while one was open for 1% -> 0% of each run, Pallas kernels for 0% -> 0%
where the time goes in v1:
time: 106 us
  Pallas kernels  100 us (94%)
  local copies, waits for them, and re-layouts  5.8 us (5%)
    pallas_call x1, Pallas kernels, per_device(): pl.pallas_call(functools.partial(fused, n_ra, n_cb), out_shape=jax.ShapeD...  100 us
    unnamed x11, local copies, waits for them, and re-layouts  5.8 us

profile of v1, /device:TPU:33, one launch (start us, length us, event | category | flops | bytes accessed | tf_op | source)
XLA Modules:
  0.0 106.2 jit_solution(18356435709866101862)
XLA Ops:
  0.0 0.0 copy-start
  0.0 1.8 %copy.10.gate1 = bf16[128,704]{1,0:T(8,128)(2,1)} copy(bf16[128,704]{0,1:T(8,128)(2,1)} %param.11) | data formatting | bytes 360448 | tf_op args[2]
  1.8 0.0 copy-done
  1.8 0.0 copy-start.1
  1.8 0.8 copy.11.up1
  2.6 0.1 copy-done.1
  2.7 0.0 copy-start.2
  2.7 0.8 copy.12.gate2
  3.5 0.1 copy-done.2
  3.6 0.8 copy.13.up2
  4.4 100.4 %shard_map.91 = bf16[128,128]{1,0:T(8,128)(2,1)} custom-call(bf16[128,128]{1,0:T(8,128)(2,1)} %tokens.1, bf16[1,128]{1,0:T(2,128)(2,1)} %bitcast.2, bf16[128,704]{1,0:T(8,128)(2,1)} %copy.10.gate1, bf16[128,704]{1,0:T(8,128)(2,1)} %copy.11.up1, bf16[704,128]{1,0:T(8,128)(2,1)} %down1.1, bf16[1,128]{1,0:T(2,128)(2,1)} %bitcast.3, ...), custom_call_target="tpu_custom_call" | custom-call | tf_op jit(solution)/shard_map/pallas_call | solution.py:137
  104.8 1.4 %copy.15 = bf16[128,128]{1,0:T(8,128)(2,1)} copy(bf16[128,128]{1,0:T(8,128)(2,1)} %shard_map.91) | data formatting | bytes 65536
Async XLA Ops:
  0.0 1.8 %copy-start = (bf16[128,704]{0,1:T(8,128)(2,1)S(1)}, bf16[128,704]{0,1:T(8,128)(2,1)}, u32[]{:S(2)}) copy-start(bf16[128,704]{0,1:T(8,128)(2,1)} %param.12) | copy-start | bytes 540676
  1.8 0.9 copy-start.1
  2.7 0.9 copy-start.2

commit v2 on v1

--- a/solution.py
+++ b/solution.py
@@ -20,12 +20,12 @@
 def fused(n_ra, n_cb, tokens, gain1, gate1, up1, down1, gain2, gate2, up2, down2, out,
           x_v, gain_v, gate_v, up_v, down_v, x_f,
           rs_out, rs_in, ag_out, ag_in, ar_in,
-          load_sem, rs_send, rs_recv, ag_send, ag_recv, ar_send, ar_recv):
+          ready, load_sem, rs_send, rs_recv, ag_send, ag_recv, ar_send, ar_recv):
     ra = lax.axis_index("ra")
     cb = lax.axis_index("cb")
     rows, cols = x_v.shape
     oct_rows = rows // n_ra
-    units = gate_v.shape[2]
+    units = gate_v.shape[1]
     half = rs_in.shape[3] // 2
     width = cols * n_ra
 
@@ -41,10 +41,18 @@
         c.start()
 
     barrier = pltpu.get_barrier_semaphore()
-    for o in far_first(n_ra):
-        pl.semaphore_signal(barrier, 1, device_id={"ra": lax.rem(ra + o, n_ra)}, device_id_type=MESH)
     for o in range(1, n_cb):
         pl.semaphore_signal(barrier, 1, device_id={"cb": lax.rem(cb + o, n_cb)}, device_id_type=MESH)
+    pl.semaphore_wait(barrier, n_cb - 1 + jnp.where(ra > 0, 1, 0))
+
+    @pl.when(ra < n_ra - 1)
+    def _():
+        pl.semaphore_signal(barrier, 1, device_id={"ra": ra + 1}, device_id_type=MESH)
+
+    for o in far_first(n_ra):
+        @pl.when(ra >= o)
+        def _():
+            pl.semaphore_signal(ready.at[o], 1, device_id={"ra": ra - o}, device_id_type=MESH)
 
     for s in range(2):
         if s == 0:
@@ -59,20 +67,27 @@
         normed = (xf * gain_v[s].astype(F32)).astype(BF16)
         pad = half - units
         for w, at, extra in ((gate_v, 0, hi), (up_v, half, sq - hi)):
-            part = jnp.dot(normed, w[s], preferred_element_type=F32)
+            part = lax.dot_general(normed, w[s], (((1,), (1,)), ((), ())), preferred_element_type=F32)
             rs_out[:, :, at:at + units] = part.reshape(n_ra, oct_rows, units).astype(BF16)
             rs_out[:, :, at + units:at + half] = jnp.broadcast_to(
                 extra.reshape(n_ra, oct_rows, 1), (n_ra, oct_rows, pad)).astype(BF16)
-        if s == 0:
-            pl.semaphore_wait(barrier, n_ra - 1 + n_cb - 1)
         sends = []
         for o in far_first(n_ra):
             to = lax.rem(ra + o, n_ra)
-            c = pltpu.make_async_remote_copy(
+            sends.append(pltpu.make_async_remote_copy(
                 src_ref=rs_out.at[to], dst_ref=rs_in.at[s, o], send_sem=rs_send.at[o],
-                recv_sem=rs_recv.at[s, o], device_id={"ra": to}, device_id_type=MESH)
-            c.start()
-            sends.append(c)
+                recv_sem=rs_recv.at[s, o], device_id={"ra": to}, device_id_type=MESH))
+        if s == 0:
+            for o, c in zip(far_first(n_ra), sends):
+                pl.when(ra + o >= n_ra)(c.start)
+            for o, c in sorted(zip(far_first(n_ra), sends), key=lambda oc: oc[0]):
+                @pl.when(ra + o < n_ra)
+                def _():
+                    pl.semaphore_wait(ready.at[o], 1)
+                    c.start()
+        else:
+            for c in sends:
+                c.start()
         total = rs_out[ra].astype(F32)
         for o in reversed(far_first(n_ra)):
             pltpu.make_async_remote_copy(
@@ -142,8 +157,8 @@
         scratch_shapes=[
             pltpu.VMEM((rows, cols), BF16),
             pltpu.VMEM((2, 1, cols), BF16),
-            pltpu.VMEM((2, cols, units), BF16),
-            pltpu.VMEM((2, cols, units), BF16),
+            pltpu.VMEM((2, units, cols), BF16),
+            pltpu.VMEM((2, units, cols), BF16),
             pltpu.VMEM((2, units, cols), BF16),
             pltpu.VMEM((rows, cols), F32),
             pltpu.VMEM((n_ra, o_rows, 2 * half), BF16),
@@ -151,14 +166,15 @@
             pltpu.VMEM((2, o_rows, units), BF16),
             pltpu.VMEM((2, n_ra, o_rows, units), BF16),
             pltpu.VMEM((2, n_cb, rows, cols), BF16),
+            pltpu.SemaphoreType.REGULAR((n_ra,)),
             dma((9,)),
             dma((n_ra,)), dma((2, n_ra)),
             dma((n_ra,)), dma((2, n_ra)),
             dma((n_cb,)), dma((2, n_cb)),
         ],
         compiler_params=pltpu.CompilerParams(collective_id=0, has_side_effects=True),
-    )(tokens, first_gain.reshape(1, -1), first_gate, first_up, first_down,
-      second_gain.reshape(1, -1), second_gate, second_up, second_down)
+    )(tokens, first_gain.reshape(1, -1), first_gate.T, first_up.T, first_down,
+      second_gain.reshape(1, -1), second_gate.T, second_up.T, second_down)
 
 
 def solution(mesh):

time: 106 us -> 108 us (1.019)
  Pallas kernels: 100 us -> 107 us
  local copies, waits for them, and re-layouts: 5.8 us -> 1.38 us
    pallas_call x1, Pallas kernels: 100 us -> 107 us  [per_device(): pl.pallas_call(functools.partial(fused, n_ra, n_cb), out_shape=jax.ShapeD...]
    unnamed x11 -> x1, local copies, waits for them, and re-layouts: 5.8 us -> 1.38 us
where the time goes in v2:
time: 108 us
  Pallas kernels  107 us (99%)
  local copies, waits for them, and re-layouts  1.38 us (1%)
    pallas_call x1, Pallas kernels, per_device(): pl.pallas_call(functools.partial(fused, n_ra, n_cb), out_shape=jax.ShapeD...  107 us

profile of v2, /device:TPU:33, one launch (start us, length us, event | category | flops | bytes accessed | tf_op | source)
XLA Modules:
  0.0 108.1 jit_solution(3827878128053346802)
XLA Ops:
  0.0 106.7 %shard_map.91 = bf16[128,128]{1,0:T(8,128)(2,1)} custom-call(bf16[128,128]{1,0:T(8,128)(2,1)} %tokens.1, bf16[1,128]{1,0:T(2,128)(2,1)} %bitcast.10, bf16[704,128]{1,0:T(8,128)(2,1)} %bitcast.6, bf16[704,128]{1,0:T(8,128)(2,1)} %bitcast.7, bf16[704,128]{1,0:T(8,128)(2,1)} %down1.1, bf16[1,128]{1,0:T(2,128)(2,1)} %bitcast.11, bf16[704,128]{1,0:T(8,128)(2,1)} %bitcast.8, ...), custom_call_target="tpu_custom_call" | custom-call | tf_op jit(solution)/shard_map/pallas_call | solution.py:152
  106.7 1.4 %copy.11 = bf16[128,128]{1,0:T(8,128)(2,1)} copy(bf16[128,128]{1,0:T(8,128)(2,1)} %shard_map.91) | data formatting | bytes 65536

commit v3 on v2

v3 whole, which is shorter than its diff:
```python
import functools

import jax
import jax.numpy as jnp
from jax import lax
from jax.experimental import pallas as pl
from jax.experimental.pallas import tpu as pltpu
from jax.sharding import PartitionSpec as P

MESH = pl.DeviceIdType.MESH
LANES = 128
BF16 = jnp.bfloat16
F32 = jnp.float32
scope = jax.named_scope
GROUPS = 4


def far_first(n):
    return sorted(range(1, n), key=lambda o: -min(o, n - o))


def groups_of(n):
    order = far_first(n) + [0]
    size = n // GROUPS
    return [order[i * size:(i + 1) * size] for i in range(GROUPS)]


def fused(n_ra, n_cb, tokens, gain1, gate1, up1, down1, gain2, gate2, up2, down2, out,
          x_v, gain_v, gate_v, up_v, down_v, x_f,
          rs_out, sums, rs_in, ag_out, ag_in, ar_in,
          ready, column, row, all_in, load_sem, rs_send, rs_recv, ag_send, ag_recv, ar_send, ar_recv):
    ra = lax.axis_index("ra")
    cb = lax.axis_index("cb")
    rows, cols = x_v.shape
    piece = rows // n_ra
    units = gate_v.shape[1]
    half = rs_in.shape[3] // 2
    width = cols * n_ra
    groups = groups_of(n_ra)

    hop = n_ra // 4
    ahead = list(range(hop + 1, n_ra // 2 + 1))
    behind = list(range(n_ra // 2 + 1, n_ra - hop))
    near = list(range(1, hop + 1)) + list(range(n_ra - hop, n_ra))

    def at(o):
        return lax.rem(ra + o, n_ra)

    loads = [pltpu.make_async_copy(tokens, x_v, load_sem.at[0])]
    for s, (gn, gt, up, dn) in enumerate(((gain1, gate1, up1, down1), (gain2, gate2, up2, down2))):
        loads += [
            pltpu.make_async_copy(gn, gain_v.at[s], load_sem.at[4 * s + 1]),
            pltpu.make_async_copy(gt, gate_v.at[s], load_sem.at[4 * s + 2]),
            pltpu.make_async_copy(up, up_v.at[s], load_sem.at[4 * s + 3]),
            pltpu.make_async_copy(dn, down_v.at[s], load_sem.at[4 * s + 4]),
        ]
    for c in loads:
        c.start()

    turn = at(n_ra - 1)
    barrier = pltpu.get_barrier_semaphore()

    @pl.when(turn == 0)
    def _():
        for o in range(1, n_cb):
            pl.semaphore_signal(barrier, 1, device_id={"cb": lax.rem(cb + o, n_cb)}, device_id_type=MESH)

    with scope("barrier"):
        pl.semaphore_wait(barrier, jnp.where(turn == 0, n_cb - 1, 1))

    @pl.when(turn < n_ra - 1)
    def _():
        pl.semaphore_signal(barrier, 1, device_id={"ra": at(1)}, device_id_type=MESH)

    for o in near:
        @pl.when(turn >= o)
        def _():
            pl.semaphore_signal(ready.at[o], 1, device_id={"ra": at(n_ra - o)}, device_id_type=MESH)

    @pl.when(turn > 0)
    def _():
        pl.semaphore_signal(column, 1, device_id={"ra": lax.rem(ra + n_ra - turn, n_ra)}, device_id_type=MESH)

    def project(s, xf, places):
        sq = jnp.sum(xf * xf, axis=1, keepdims=True)
        hi = sq.astype(BF16).astype(F32)
        normed = (xf * gain_v[s].astype(F32)).astype(BF16)
        for w, lane, extra in ((gate_v, 0, hi), (up_v, half, sq - hi)):
            part = lax.dot_general(normed, w[s], (((1,), (1,)), ((), ())), preferred_element_type=F32)
            for i, place in enumerate(places):
                cut = slice(i * piece, (i + 1) * piece)
                rs_out[s, place, :, lane:lane + units] = part[cut].astype(BF16)
                rs_out[s, place, :, lane + units:lane + half] = jnp.broadcast_to(
                    extra[cut], (piece, half - units)).astype(BF16)

    def scatter(s):
        def ring(src, o, to):
            return pltpu.make_async_remote_copy(
                src_ref=src, dst_ref=rs_in.at[s, o], send_sem=rs_send.at[s, o], recv_sem=rs_recv.at[s, o],
                device_id={"ra": at(to)}, device_id_type=MESH)

        copies = {o: ring(rs_out.at[s, at(o)], o, o) for o in near if o not in (hop, n_ra - hop)}
        copies |= {o: ring(rs_out.at[s, at(o)], o, o - hop) for o in ahead}
        copies |= {o: ring(rs_out.at[s, at(o)], o, o + hop) for o in behind}
        copies |= {o: ring(sums.at[s, i], o, o) for i, o in enumerate((n_ra - hop, hop))}
        return copies

    def via(o):
        return o - hop if o in ahead else o + hop if o in behind else o

    def ag_copy(s, o, slot):
        return pltpu.make_async_remote_copy(
            src_ref=ag_out.at[s], dst_ref=ag_in.at[s, slot], send_sem=ag_send.at[s, o],
            recv_sem=ag_recv.at[s, o], device_id={"ra": at(o)}, device_id_type=MESH)

    def ar_copy(s, g, o, slot):
        return pltpu.make_async_remote_copy(
            src_ref=ar_in.at[s, g, cb], dst_ref=ar_in.at[s, g, slot], send_sem=ar_send.at[s, g, o],
            recv_sem=ar_recv.at[s, g, o], device_id={"cb": lax.rem(cb + o, n_cb)}, device_id_type=MESH)

    rs = [scatter(s) for s in range(2)]
    relays = (n_ra - hop, hop)
    free = [o for o in far_first(n_ra) if o not in relays]

    with scope("load"):
        for c in loads[:4]:
            c.wait()
    with scope("project_first"):
        xf = x_v[...].astype(F32)
        for i in range(n_ra):
            x_f[i] = xf[i * piece:(i + 1) * piece]
        project(0, xf, range(n_ra))
    with scope("send_first"):
        for o in free:
            pl.when(turn + via(o) >= n_ra)(rs[0][o].start)
    with scope("send_ready"):
        for p in near:
            @pl.when(turn + p < n_ra)
            def _():
                pl.semaphore_wait(ready.at[p], 1)
                for o in free:
                    if via(o) == p:
                        rs[0][o].start()

    @pl.when(turn == 0)
    def _():
        pl.semaphore_wait(column, n_ra - 1)
        for o in range(1, n_cb):
            pl.semaphore_signal(row, 1, device_id={"cb": lax.rem(cb + o, n_cb)}, device_id_type=MESH)
        pl.semaphore_wait(row, n_cb - 1)
        for o in far_first(n_ra):
            pl.semaphore_signal(all_in, 1, device_id={"ra": at(o)}, device_id_type=MESH)

    for s in range(2):
        for i, (o, far) in enumerate(zip(relays, (behind, ahead))):
            part = rs_out[s, at(o)].astype(F32)
            for f in far:
                with scope(f"relay_wait{s}_{f}"):
                    rs[s][f].wait_recv()
                part = part + rs_in[s, f].astype(F32)
            sums[s, i] = part.astype(BF16)
            rs[s][o].start()
        total = rs_out[s, ra].astype(F32)
        for o in sorted(near, key=lambda o: min(o, n_ra - o)):
            with scope(f"scatter_wait{s}_{o}"):
                rs[s][o].wait_recv()
            total = total + rs_in[s, o].astype(F32)
        sumsq = total[:, units:units + 1] + total[:, half + units:half + units + 1]
        scale = lax.rsqrt(sumsq / width + 1e-06)
        g = total[:, :units] * scale
        hidden = (g / (1.0 + jnp.exp(-g)) * (total[:, half:half + units] * scale)).astype(BF16)
        ag_out[s] = hidden
        ag_in[s, ra] = hidden
        ag = [ag_copy(s, o, ra) for o in far_first(n_ra)]
        for c in ag:
            c.start()
        loads[4 * s + 4].wait()
        for c in rs[s].values():
            c.wait_send()
        if s == 0:
            for c in loads[5:8]:
                c.wait()

        ar = []

        def down(g):
            for o in groups[g]:
                if o:
                    with scope(f"gather_wait{s}_{o}"):
                        ag_copy(s, n_ra - o, at(o)).wait_recv()
            h = jnp.concatenate([ag_in[s, at(o)].astype(F32) for o in groups[g]], axis=0).astype(BF16)
            ar_in[s, g, cb] = jnp.dot(h, down_v[s], preferred_element_type=F32).astype(BF16)
            for o in far_first(n_cb):
                c = ar_copy(s, g, o, cb)
                c.start()
                ar.append(c)

        def finish(g):
            with scope(f"cb_wait{s}_{g}"):
                for o in far_first(n_cb):
                    ar_copy(s, g, o, lax.rem(cb + n_cb - o, n_cb)).wait_recv()
            branch = ar_in[s, g, 0].astype(F32)
            for c in range(1, n_cb):
                branch = branch + ar_in[s, g, c].astype(F32)
            places = [at(o) for o in groups[g]]
            old = jnp.concatenate([x_f[p] for p in places], axis=0)
            result = (0.5 * old + 0.5 * branch).astype(BF16)
            if s == 1:
                for i, p in enumerate(places):
                    out[p] = result[i * piece:(i + 1) * piece]
                return
            new = result.astype(F32)
            for i, p in enumerate(places):
                x_f[p] = new[i * piece:(i + 1) * piece]
            project(1, new, places)
            for o in groups[g]:
                if o in free:
                    rs[1][o].start()

        if s == 0:
            with scope("all_in"):
                @pl.when(turn > 0)
                def _():
                    pl.semaphore_wait(all_in, 1)
        for g in range(GROUPS):
            down(g)
        for c in ag:
            c.wait_send()
        for g in range(GROUPS):
            finish(g)
        for c in ar:
            c.wait_send()


def per_device(tokens, first_gain, first_gate, first_up, first_down,
               second_gain, second_gate, second_up, second_down):
    n_ra, n_cb = lax.axis_size("ra"), lax.axis_size("cb")
    rows, cols = tokens.shape
    units = first_gate.shape[1]
    half = (units // LANES + 1) * LANES
    piece = rows // n_ra
    dma = pltpu.SemaphoreType.DMA
    any_spec = pl.BlockSpec(memory_space=pl.ANY)
    out = pl.pallas_call(
        functools.partial(fused, n_ra, n_cb),
        out_shape=jax.ShapeDtypeStruct((n_ra, piece, cols), BF16),
        in_specs=[any_spec] * 9,
        out_specs=pl.BlockSpec(memory_space=pltpu.VMEM),
        scratch_shapes=[
            pltpu.VMEM((rows, cols), BF16),
            pltpu.VMEM((2, 1, cols), BF16),
            pltpu.VMEM((2, units, cols), BF16),
            pltpu.VMEM((2, units, cols), BF16),
            pltpu.VMEM((2, units, cols), BF16),
            pltpu.VMEM((n_ra, piece, cols), F32),
            pltpu.VMEM((2, n_ra, piece, 2 * half), BF16),
            pltpu.VMEM((2, 2, piece, 2 * half), BF16),
            pltpu.VMEM((2, n_ra, piece, 2 * half), BF16),
            pltpu.VMEM((2, piece, units), BF16),
            pltpu.VMEM((2, n_ra, piece, units), BF16),
            pltpu.VMEM((2, GROUPS, n_cb, rows // GROUPS, cols), BF16),
            pltpu.SemaphoreType.REGULAR((n_ra,)),
            pltpu.SemaphoreType.REGULAR,
            pltpu.SemaphoreType.REGULAR,
            pltpu.SemaphoreType.REGULAR,
            dma((9,)),
            dma((2, n_ra)), dma((2, n_ra)),
            dma((2, n_ra)), dma((2, n_ra)),
            dma((2, GROUPS, n_cb)), dma((2, GROUPS, n_cb)),
        ],
        compiler_params=pltpu.CompilerParams(collective_id=0, has_side_effects=True),
    )(tokens, first_gain.reshape(1, -1), first_gate.T, first_up.T, first_down,
      second_gain.reshape(1, -1), second_gate.T, second_up.T, second_down)
    return out.reshape(rows, cols)


def solution(mesh):
    placed = (
        P("grp", "ra"),
        P("ra"), P("ra", "cb"), P("ra", "cb"), P("cb", "ra"),
        P("ra"), P("ra", "cb"), P("ra", "cb"), P("cb", "ra"),
    )
    return jax.shard_map(
        per_device, mesh=mesh, in_specs=placed, out_specs=P("grp", "ra"), check_vma=False
    )
```

time: 108 us -> 87.6 us (0.81)
  Pallas kernels: 107 us -> 86.1 us
    pallas_call x1, Pallas kernels: 107 us -> 86.1 us  [per_device(): pl.pallas_call(functools.partial(fused, n_ra, n_cb), out_shape=jax.ShapeD...]
where the time goes in v3:
time: 87.6 us; the launch traced here: 87.5 us
  Pallas kernels  86.1 us (98%)
  local copies, waits for them, and re-layouts  1.38 us (2%)
    pallas_call x1, Pallas kernels, per_device(): pl.pallas_call(functools.partial(fused, n_ra, n_cb), out_shape=jax.ShapeD...  86.1 us

profile of v3, /device:TPU:33, one launch (start us, length us, event | category | flops | bytes accessed | tf_op | source)
XLA Modules:
  0.0 87.5 jit_solution(6335093974421900642)
XLA Ops:
  0.0 86.1 %shard_map.91 = bf16[16,8,128]{2,1,0:T(8,128)(2,1)} custom-call(bf16[128,128]{1,0:T(8,128)(2,1)} %tokens.1, bf16[1,128]{1,0:T(2,128)(2,1)} %bitcast.12, bf16[704,128]{1,0:T(8,128)(2,1)} %bitcast.7, bf16[704,128]{1,0:T(8,128)(2,1)} %bitcast.8, bf16[704,128]{1,0:T(8,128)(2,1)} %down1.1, bf16[1,128]{1,0:T(2,128)(2,1)} %bitcast.13, bf16[704,128]{1,0:T(8,128)(2,1)} %bitcast.9, ...), custom_call_target="tpu_custom_call" | custom-call | tf_op jit(solution)/shard_map/pallas_call | solution.py:244
  86.1 1.4 %copy.11 = bf16[128,128]{1,0:T(8,128)(2,1)} copy(bf16[128,128]{1,0:T(8,128)(2,1)} %bitcast.11) | data formatting | bytes 65536

commit v4 on v3

--- a/solution.py
+++ b/solution.py
@@ -12,7 +12,7 @@
 BF16 = jnp.bfloat16
 F32 = jnp.float32
 scope = jax.named_scope
-GROUPS = 4
+GROUPS = (4, 4)
 
 
 def far_first(n):
@@ -21,13 +21,12 @@
 
 def groups_of(n):
     order = far_first(n) + [0]
-    size = n // GROUPS
-    return [order[i * size:(i + 1) * size] for i in range(GROUPS)]
+    return [[order[i:i + n // k] for i in range(0, n, n // k)] for k in GROUPS]
 
 
 def fused(n_ra, n_cb, tokens, gain1, gate1, up1, down1, gain2, gate2, up2, down2, out,
           x_v, gain_v, gate_v, up_v, down_v, x_f,
-          rs_out, sums, rs_in, ag_out, ag_in, ar_in,
+          rs_out, sums, rs_in, ag_out, ag_in, ar_in1, ar_in2,
           ready, column, row, all_in, load_sem, rs_send, rs_recv, ag_send, ag_recv, ar_send, ar_recv):
     ra = lax.axis_index("ra")
     cb = lax.axis_index("cb")
@@ -36,12 +35,15 @@
     units = gate_v.shape[1]
     half = rs_in.shape[3] // 2
     width = cols * n_ra
-    groups = groups_of(n_ra)
+    ar_ins = (ar_in1, ar_in2)
+    all_groups = groups_of(n_ra)
 
     hop = n_ra // 4
     ahead = list(range(hop + 1, n_ra // 2 + 1))
     behind = list(range(n_ra // 2 + 1, n_ra - hop))
     near = list(range(1, hop + 1)) + list(range(n_ra - hop, n_ra))
+
+    relays = (n_ra - hop, hop)
 
     def at(o):
         return lax.rem(ra + o, n_ra)
@@ -57,7 +59,13 @@
     for c in loads:
         c.start()
 
-    turn = at(n_ra - 1)
+    turn = lax.rem(ra + n_ra - 1, n_ra)
+    odd = lax.rem(cb, 2) == 1
+    partner = {"cb": cb + 1 - 2 * lax.rem(cb, 2)}
+
+    def later(o):
+        return turn + o < n_ra
+
     barrier = pltpu.get_barrier_semaphore()
 
     @pl.when(turn == 0)
@@ -65,17 +73,25 @@
         for o in range(1, n_cb):
             pl.semaphore_signal(barrier, 1, device_id={"cb": lax.rem(cb + o, n_cb)}, device_id_type=MESH)
 
+    @pl.when(jnp.logical_and(turn > 0, jnp.logical_not(odd)))
+    def _():
+        pl.semaphore_signal(barrier, 1, device_id=partner, device_id_type=MESH)
+
     with scope("barrier"):
-        pl.semaphore_wait(barrier, jnp.where(turn == 0, n_cb - 1, 1))
-
-    @pl.when(turn < n_ra - 1)
-    def _():
-        pl.semaphore_signal(barrier, 1, device_id={"ra": at(1)}, device_id_type=MESH)
+        pl.semaphore_wait(barrier, jnp.where(turn == 0, n_cb - 1, jnp.where(odd, 2, 1)))
+
+    @pl.when(jnp.logical_and(turn < n_ra - 1, odd))
+    def _():
+        pl.semaphore_signal(barrier, 1, device_id={"ra": lax.rem(ra + 1, n_ra)}, device_id_type=MESH)
+
+    @pl.when(jnp.logical_and(turn > 0, odd))
+    def _():
+        pl.semaphore_signal(barrier, 1, device_id=partner, device_id_type=MESH)
 
     for o in near:
         @pl.when(turn >= o)
         def _():
-            pl.semaphore_signal(ready.at[o], 1, device_id={"ra": at(n_ra - o)}, device_id_type=MESH)
+            pl.semaphore_signal(ready.at[near.index(o)], 1, device_id={"ra": at(n_ra - o)}, device_id_type=MESH)
 
     @pl.when(turn > 0)
     def _():
@@ -93,10 +109,21 @@
                 rs_out[s, place, :, lane + units:lane + half] = jnp.broadcast_to(
                     extra[cut], (piece, half - units)).astype(BF16)
 
+    def batch(o):
+        return 0 if o in ahead else 1 if o in behind else 2 if o == hop else 3 if o == n_ra - hop else 4
+
+    def all_of(ref, send_sem, recv_sem):
+        return pltpu.make_async_remote_copy(
+            src_ref=ref, dst_ref=ref, send_sem=send_sem, recv_sem=recv_sem,
+            device_id={"ra": at(1)}, device_id_type=MESH)
+
+    def scattered(s, count, which=0):
+        return all_of(rs_in.at[s, pl.ds(0, count)], rs_send.at[s], rs_recv.at[s, which])
+
     def scatter(s):
         def ring(src, o, to):
             return pltpu.make_async_remote_copy(
-                src_ref=src, dst_ref=rs_in.at[s, o], send_sem=rs_send.at[s, o], recv_sem=rs_recv.at[s, o],
+                src_ref=src, dst_ref=rs_in.at[s, o], send_sem=rs_send.at[s], recv_sem=rs_recv.at[s, batch(o)],
                 device_id={"ra": at(to)}, device_id_type=MESH)
 
         copies = {o: ring(rs_out.at[s, at(o)], o, o) for o in near if o not in (hop, n_ra - hop)}
@@ -108,18 +135,20 @@
     def via(o):
         return o - hop if o in ahead else o + hop if o in behind else o
 
-    def ag_copy(s, o, slot):
+    def ag_copy(s, o):
+        seen = n_ra - o
+        group = [seen in g for g in all_groups[s]].index(True)
         return pltpu.make_async_remote_copy(
-            src_ref=ag_out.at[s], dst_ref=ag_in.at[s, slot], send_sem=ag_send.at[s, o],
-            recv_sem=ag_recv.at[s, o], device_id={"ra": at(o)}, device_id_type=MESH)
-
-    def ar_copy(s, g, o, slot):
-        return pltpu.make_async_remote_copy(
-            src_ref=ar_in.at[s, g, cb], dst_ref=ar_in.at[s, g, slot], send_sem=ar_send.at[s, g, o],
-            recv_sem=ar_recv.at[s, g, o], device_id={"cb": lax.rem(cb + o, n_cb)}, device_id_type=MESH)
+            src_ref=ag_out.at[s], dst_ref=ag_in.at[s, ra], send_sem=ag_send.at[s],
+            recv_sem=ag_recv.at[s, group], device_id={"ra": at(o)}, device_id_type=MESH)
+
+    def gathered(s, count, recv_sem):
+        return all_of(ag_in.at[s, pl.ds(0, count)], ag_send.at[s], recv_sem)
+
+    def summed(s, g):
+        return all_of(ar_ins[s].at[g, pl.ds(0, n_cb - 1)], ar_send.at[s, g], ar_recv.at[s, g])
 
     rs = [scatter(s) for s in range(2)]
-    relays = (n_ra - hop, hop)
     free = [o for o in far_first(n_ra) if o not in relays]
 
     with scope("load"):
@@ -132,12 +161,12 @@
         project(0, xf, range(n_ra))
     with scope("send_first"):
         for o in free:
-            pl.when(turn + via(o) >= n_ra)(rs[0][o].start)
+            pl.when(jnp.logical_not(later(via(o))))(rs[0][o].start)
     with scope("send_ready"):
         for p in near:
-            @pl.when(turn + p < n_ra)
+            @pl.when(later(p))
             def _():
-                pl.semaphore_wait(ready.at[p], 1)
+                pl.semaphore_wait(ready.at[near.index(p)], 1)
                 for o in free:
                     if via(o) == p:
                         rs[0][o].start()
@@ -154,16 +183,21 @@
     for s in range(2):
         for i, (o, far) in enumerate(zip(relays, (behind, ahead))):
             part = rs_out[s, at(o)].astype(F32)
+            with scope(f"relay_wait{s}_{o}"):
+                scattered(s, len(far), batch(far[0])).wait_recv()
             for f in far:
-                with scope(f"relay_wait{s}_{f}"):
-                    rs[s][f].wait_recv()
                 part = part + rs_in[s, f].astype(F32)
             sums[s, i] = part.astype(BF16)
             rs[s][o].start()
         total = rs_out[s, ra].astype(F32)
-        for o in sorted(near, key=lambda o: min(o, n_ra - o)):
+        direct = [o for o in near if o not in relays]
+        with scope(f"scatter_wait{s}_direct"):
+            scattered(s, len(direct), batch(direct[0])).wait_recv()
+        for o in direct:
+            total = total + rs_in[s, o].astype(F32)
+        for o in relays:
             with scope(f"scatter_wait{s}_{o}"):
-                rs[s][o].wait_recv()
+                scattered(s, 1, batch(o)).wait_recv()
             total = total + rs_in[s, o].astype(F32)
         sumsq = total[:, units:units + 1] + total[:, half + units:half + units + 1]
         scale = lax.rsqrt(sumsq / width + 1e-06)
@@ -171,37 +205,40 @@
         hidden = (g / (1.0 + jnp.exp(-g)) * (total[:, half:half + units] * scale)).astype(BF16)
         ag_out[s] = hidden
         ag_in[s, ra] = hidden
-        ag = [ag_copy(s, o, ra) for o in far_first(n_ra)]
-        for c in ag:
-            c.start()
+        ag = [ag_copy(s, o) for o in far_first(n_ra)]
+        if s == 1:
+            for early in (True, False):
+                for o, c in zip(far_first(n_ra), ag):
+                    pl.when((at(o) < n_ra // 2) == early)(c.start)
+        else:
+            for c in ag:
+                c.start()
         loads[4 * s + 4].wait()
-        for c in rs[s].values():
-            c.wait_send()
+        scattered(s, n_ra - 1).wait_send()
         if s == 0:
             for c in loads[5:8]:
                 c.wait()
 
-        ar = []
+        groups = all_groups[s]
+        ar_in = ar_ins[s]
 
         def down(g):
-            for o in groups[g]:
-                if o:
-                    with scope(f"gather_wait{s}_{o}"):
-                        ag_copy(s, n_ra - o, at(o)).wait_recv()
+            with scope(f"gather_wait{s}_{g}"):
+                count = sum(o != 0 for o in groups[g])
+                gathered(s, count, ag_recv.at[s, g]).wait_recv()
             h = jnp.concatenate([ag_in[s, at(o)].astype(F32) for o in groups[g]], axis=0).astype(BF16)
-            ar_in[s, g, cb] = jnp.dot(h, down_v[s], preferred_element_type=F32).astype(BF16)
+            ar_in[g, cb] = jnp.dot(h, down_v[s], preferred_element_type=F32).astype(BF16)
             for o in far_first(n_cb):
-                c = ar_copy(s, g, o, cb)
-                c.start()
-                ar.append(c)
+                pltpu.make_async_remote_copy(
+                    src_ref=ar_in.at[g, cb], dst_ref=ar_in.at[g, cb], send_sem=ar_send.at[s, g],
+                    recv_sem=ar_recv.at[s, g], device_id={"cb": lax.rem(cb + o, n_cb)}, device_id_type=MESH).start()
 
         def finish(g):
             with scope(f"cb_wait{s}_{g}"):
-                for o in far_first(n_cb):
-                    ar_copy(s, g, o, lax.rem(cb + n_cb - o, n_cb)).wait_recv()
-            branch = ar_in[s, g, 0].astype(F32)
+                summed(s, g).wait_recv()
+            branch = ar_in[g, 0].astype(F32)
             for c in range(1, n_cb):
-                branch = branch + ar_in[s, g, c].astype(F32)
+                branch = branch + ar_in[g, c].astype(F32)
             places = [at(o) for o in groups[g]]
             old = jnp.concatenate([x_f[p] for p in places], axis=0)
             result = (0.5 * old + 0.5 * branch).astype(BF16)
@@ -222,14 +259,13 @@
                 @pl.when(turn > 0)
                 def _():
                     pl.semaphore_wait(all_in, 1)
-        for g in range(GROUPS):
+        for g in range(len(groups)):
             down(g)
-        for c in ag:
-            c.wait_send()
-        for g in range(GROUPS):
+        gathered(s, n_ra - 1, ag_recv.at[s, 0]).wait_send()
+        for g in range(len(groups)):
             finish(g)
-        for c in ar:
-            c.wait_send()
+        for g in range(len(groups)):
+            summed(s, g).wait_send()
 
 
 def per_device(tokens, first_gain, first_gate, first_up, first_down,
@@ -243,7 +279,7 @@
     any_spec = pl.BlockSpec(memory_space=pl.ANY)
     out = pl.pallas_call(
         functools.partial(fused, n_ra, n_cb),
-        out_shape=jax.ShapeDtypeStruct((n_ra, piece, cols), BF16),
+        out_shape=pltpu.VMEM((n_ra, piece, cols), BF16),
         in_specs=[any_spec] * 9,
         out_specs=pl.BlockSpec(memory_space=pltpu.VMEM),
         scratch_shapes=[
@@ -258,15 +294,15 @@
             pltpu.VMEM((2, n_ra, piece, 2 * half), BF16),
             pltpu.VMEM((2, piece, units), BF16),
             pltpu.VMEM((2, n_ra, piece, units), BF16),
-            pltpu.VMEM((2, GROUPS, n_cb, rows // GROUPS, cols), BF16),
-            pltpu.SemaphoreType.REGULAR((n_ra,)),
+            *(pltpu.VMEM((k, n_cb, rows // k, cols), BF16) for k in GROUPS),
+            pltpu.SemaphoreType.REGULAR((n_ra // 2,)),
             pltpu.SemaphoreType.REGULAR,
             pltpu.SemaphoreType.REGULAR,
             pltpu.SemaphoreType.REGULAR,
             dma((9,)),
-            dma((2, n_ra)), dma((2, n_ra)),
-            dma((2, n_ra)), dma((2, n_ra)),
-            dma((2, GROUPS, n_cb)), dma((2, GROUPS, n_cb)),
+            dma((2,)), dma((2, 5)),
+            dma((2,)), dma((2, max(GROUPS))),
+            dma((2, max(GROUPS))), dma((2, max(GROUPS))),
         ],
         compiler_params=pltpu.CompilerParams(collective_id=0, has_side_effects=True),
     )(tokens, first_gain.reshape(1, -1), first_gate.T, first_up.T, first_down,

time: 87.6 us -> 83.7 us (0.955)
  Pallas kernels: 86.1 us -> 83 us
    pallas_call x1, Pallas kernels: 86.1 us -> 83 us  [per_device(): pl.pallas_call(functools.partial(fused, n_ra, n_cb), out_shape=pltpu.VMEM...]
where the time goes in v4:
time: 83.7 us; the launch traced here: 83.6 us
  Pallas kernels  83 us (99%)
    pallas_call x1, Pallas kernels, per_device(): pl.pallas_call(functools.partial(fused, n_ra, n_cb), out_shape=pltpu.VMEM...  83 us

profile of v4, /device:TPU:33, one launch (start us, length us, event | category | flops | bytes accessed | tf_op | source)
XLA Modules:
  0.0 83.6 jit_solution(17145348079098696429)
XLA Ops:
  0.0 83.0 %shard_map.91 = bf16[16,8,128]{2,1,0:T(8,128)(2,1)S(1)} custom-call(bf16[128,128]{1,0:T(8,128)(2,1)} %tokens.1, bf16[1,128]{1,0:T(2,128)(2,1)} %bitcast.12, bf16[704,128]{1,0:T(8,128)(2,1)} %bitcast.8, bf16[704,128]{1,0:T(8,128)(2,1)} %bitcast.9, bf16[704,128]{1,0:T(8,128)(2,1)} %down1.1, bf16[1,128]{1,0:T(2,128)(2,1)} %bitcast.13, ...), custom_call_target="tpu_custom_call" | custom-call | tf_op jit(solution)/shard_map/pallas_call | solution.py:280
  83.0 0.6 copy.11

commit v5 on v4

--- a/solution.py
+++ b/solution.py
@@ -12,7 +12,7 @@
 BF16 = jnp.bfloat16
 F32 = jnp.float32
 scope = jax.named_scope
-GROUPS = (4, 4)
+GROUPS = (8, 4)
 
 
 def far_first(n):

time: 83.7 us -> 82.8 us (0.989)
  Pallas kernels: 83 us -> 82.1 us
where the time goes in v5:
time: 82.8 us
  Pallas kernels  82.1 us (99%)
    pallas_call x1, Pallas kernels, per_device(): pl.pallas_call(functools.partial(fused, n_ra, n_cb), out_shape=pltpu.VMEM...  82.1 us

profile of v5, /device:TPU:33, one launch (start us, length us, event | category | flops | bytes accessed | tf_op | source)
XLA Modules:
  0.0 82.8 jit_solution(12241361569734628212)
XLA Ops:
  0.0 82.1 %shard_map.91 = bf16[16,8,128]{2,1,0:T(8,128)(2,1)S(1)} custom-call(bf16[128,128]{1,0:T(8,128)(2,1)} %tokens.1, bf16[1,128]{1,0:T(2,128)(2,1)} %bitcast.12, bf16[704,128]{1,0:T(8,128)(2,1)} %bitcast.8, bf16[704,128]{1,0:T(8,128)(2,1)} %bitcast.9, bf16[704,128]{1,0:T(8,128)(2,1)} %down1.1, bf16[1,128]{1,0:T(2,128)(2,1)} %bitcast.13, ...), custom_call_target="tpu_custom_call" | custom-call | tf_op jit(solution)/shard_map/pallas_call | solution.py:280
  82.1 0.6 copy.11

commit v6 on v5

--- a/solution.py
+++ b/solution.py
@@ -26,14 +26,16 @@
 
 def fused(n_ra, n_cb, tokens, gain1, gate1, up1, down1, gain2, gate2, up2, down2, out,
           x_v, gain_v, gate_v, up_v, down_v, x_f,
-          rs_out, sums, rs_in, ag_out, ag_in, ar_in1, ar_in2,
-          ready, column, row, all_in, load_sem, rs_send, rs_recv, ag_send, ag_recv, ar_send, ar_recv):
+          rs_out, sums, rs_in, sq_out, sq_sums, sq_in, ag_out, ag_in, ar_in1, ar_in2,
+          ready, column, row, all_in, load_sem, rs_send, rs_recv, sq_send, sq_recv, ag_send, ag_recv, ar_send, ar_recv):
     ra = lax.axis_index("ra")
     cb = lax.axis_index("cb")
     rows, cols = x_v.shape
     piece = rows // n_ra
     units = gate_v.shape[1]
-    half = rs_in.shape[3] // 2
+    main = units // LANES * LANES
+    rest = units - main
+    diagonal = lax.broadcasted_iota(jnp.int32, (piece, LANES), 0) == lax.broadcasted_iota(jnp.int32, (piece, LANES), 1)
     width = cols * n_ra
     ar_ins = (ar_in1, ar_in2)
     all_groups = groups_of(n_ra)
@@ -99,15 +101,17 @@
 
     def project(s, xf, places):
         sq = jnp.sum(xf * xf, axis=1, keepdims=True)
-        hi = sq.astype(BF16).astype(F32)
         normed = (xf * gain_v[s].astype(F32)).astype(BF16)
-        for w, lane, extra in ((gate_v, 0, hi), (up_v, half, sq - hi)):
-            part = lax.dot_general(normed, w[s], (((1,), (1,)), ((), ())), preferred_element_type=F32)
-            for i, place in enumerate(places):
-                cut = slice(i * piece, (i + 1) * piece)
-                rs_out[s, place, :, lane:lane + units] = part[cut].astype(BF16)
-                rs_out[s, place, :, lane + units:lane + half] = jnp.broadcast_to(
-                    extra[cut], (piece, half - units)).astype(BF16)
+        gate, up = (
+            lax.dot_general(normed, w[s], (((1,), (1,)), ((), ())), preferred_element_type=F32)
+            for w in (gate_v, up_v))
+        ends = jnp.concatenate([gate[:, main:], up[:, main:]], axis=1)
+        for i, place in enumerate(places):
+            cut = slice(i * piece, (i + 1) * piece)
+            rs_out[s, place, :, :main] = gate[cut, :main].astype(BF16)
+            rs_out[s, place, :, main:2 * main] = up[cut, :main].astype(BF16)
+            rs_out[s, place, :, 2 * main:2 * units] = ends[cut].astype(BF16)
+            sq_out[s, place] = jnp.sum(jnp.where(diagonal, sq[cut], 0.0), axis=0, keepdims=True)
 
     def batch(o):
         return 0 if o in ahead else 1 if o in behind else 2 if o == hop else 3 if o == n_ra - hop else 4
@@ -118,18 +122,36 @@
             device_id={"ra": at(1)}, device_id_type=MESH)
 
     def scattered(s, count, which=0):
-        return all_of(rs_in.at[s, pl.ds(0, count)], rs_send.at[s], rs_recv.at[s, which])
+        return (
+            all_of(rs_in.at[s, pl.ds(0, count)], rs_send.at[s], rs_recv.at[s, which]),
+            all_of(sq_in.at[s, pl.ds(0, count)], sq_send.at[s], sq_recv.at[s, which]))
+
+    def arrived(s, count, which):
+        for c in scattered(s, count, which):
+            c.wait_recv()
 
     def scatter(s):
-        def ring(src, o, to):
-            return pltpu.make_async_remote_copy(
-                src_ref=src, dst_ref=rs_in.at[s, o], send_sem=rs_send.at[s], recv_sem=rs_recv.at[s, batch(o)],
-                device_id={"ra": at(to)}, device_id_type=MESH)
-
-        copies = {o: ring(rs_out.at[s, at(o)], o, o) for o in near if o not in (hop, n_ra - hop)}
-        copies |= {o: ring(rs_out.at[s, at(o)], o, o - hop) for o in ahead}
-        copies |= {o: ring(rs_out.at[s, at(o)], o, o + hop) for o in behind}
-        copies |= {o: ring(sums.at[s, i], o, o) for i, o in enumerate((n_ra - hop, hop))}
+        def ring(src, src_sq, o, to):
+            both = [
+                pltpu.make_async_remote_copy(
+                    src_ref=ref, dst_ref=dst.at[s, o], send_sem=send.at[s], recv_sem=recv.at[s, batch(o)],
+                    device_id={"ra": at(to)}, device_id_type=MESH)
+                for ref, dst, send, recv in (
+                    (src_sq, sq_in, sq_send, sq_recv), (src, rs_in, rs_send, rs_recv))]
+
+            def start():
+                for c in both:
+                    c.start()
+
+            return start
+
+        def term(o, to):
+            return ring(rs_out.at[s, at(o)], sq_out.at[s, at(o)], o, to)
+
+        copies = {o: term(o, o) for o in near if o not in relays}
+        copies |= {o: term(o, o - hop) for o in ahead}
+        copies |= {o: term(o, o + hop) for o in behind}
+        copies |= {o: ring(sums.at[s, i], sq_sums.at[s, i], o, o) for i, o in enumerate(relays)}
         return copies
 
     def via(o):
@@ -161,7 +183,7 @@
         project(0, xf, range(n_ra))
     with scope("send_first"):
         for o in free:
-            pl.when(jnp.logical_not(later(via(o))))(rs[0][o].start)
+            pl.when(jnp.logical_not(later(via(o))))(rs[0][o])
     with scope("send_ready"):
         for p in near:
             @pl.when(later(p))
@@ -169,7 +191,7 @@
                 pl.semaphore_wait(ready.at[near.index(p)], 1)
                 for o in free:
                     if via(o) == p:
-                        rs[0][o].start()
+                        rs[0][o]()
 
     @pl.when(turn == 0)
     def _():
@@ -184,37 +206,46 @@
         for i, (o, far) in enumerate(zip(relays, (behind, ahead))):
             part = rs_out[s, at(o)].astype(F32)
             with scope(f"relay_wait{s}_{o}"):
-                scattered(s, len(far), batch(far[0])).wait_recv()
+                arrived(s, len(far), batch(far[0]))
+            part_sq = sq_out[s, at(o)]
             for f in far:
                 part = part + rs_in[s, f].astype(F32)
+                part_sq = part_sq + sq_in[s, f]
             sums[s, i] = part.astype(BF16)
-            rs[s][o].start()
+            sq_sums[s, i] = part_sq
+            rs[s][o]()
         total = rs_out[s, ra].astype(F32)
         direct = [o for o in near if o not in relays]
         with scope(f"scatter_wait{s}_direct"):
-            scattered(s, len(direct), batch(direct[0])).wait_recv()
+            arrived(s, len(direct), batch(direct[0]))
+        total_sq = sq_out[s, ra]
         for o in direct:
             total = total + rs_in[s, o].astype(F32)
+            total_sq = total_sq + sq_in[s, o]
         for o in relays:
             with scope(f"scatter_wait{s}_{o}"):
-                scattered(s, 1, batch(o)).wait_recv()
+                arrived(s, 1, batch(o))
             total = total + rs_in[s, o].astype(F32)
-        sumsq = total[:, units:units + 1] + total[:, half + units:half + units + 1]
+            total_sq = total_sq + sq_in[s, o]
+        sumsq = jnp.sum(jnp.where(diagonal, total_sq, 0.0), axis=1, keepdims=True)
         scale = lax.rsqrt(sumsq / width + 1e-06)
-        g = total[:, :units] * scale
-        hidden = (g / (1.0 + jnp.exp(-g)) * (total[:, half:half + units] * scale)).astype(BF16)
+        ends = total[:, 2 * main:2 * units]
+        g = jnp.concatenate([total[:, :main], ends[:, :rest]], axis=1) * scale
+        u = jnp.concatenate([total[:, main:2 * main], ends[:, rest:]], axis=1) * scale
+        hidden = (g / (1.0 + jnp.exp(-g)) * u).astype(BF16)
         ag_out[s] = hidden
         ag_in[s, ra] = hidden
         ag = [ag_copy(s, o) for o in far_first(n_ra)]
         if s == 1:
-            for early in (True, False):
+            for tier in range(4):
                 for o, c in zip(far_first(n_ra), ag):
-                    pl.when((at(o) < n_ra // 2) == early)(c.start)
+                    pl.when(at(o) // (n_ra // 4) == tier)(c.start)
         else:
             for c in ag:
                 c.start()
         loads[4 * s + 4].wait()
-        scattered(s, n_ra - 1).wait_send()
+        for c in scattered(s, n_ra - 1):
+            c.wait_send()
         if s == 0:
             for c in loads[5:8]:
                 c.wait()
@@ -252,7 +283,7 @@
             project(1, new, places)
             for o in groups[g]:
                 if o in free:
-                    rs[1][o].start()
+                    rs[1][o]()
 
         if s == 0:
             with scope("all_in"):
@@ -273,7 +304,6 @@
     n_ra, n_cb = lax.axis_size("ra"), lax.axis_size("cb")
     rows, cols = tokens.shape
     units = first_gate.shape[1]
-    half = (units // LANES + 1) * LANES
     piece = rows // n_ra
     dma = pltpu.SemaphoreType.DMA
     any_spec = pl.BlockSpec(memory_space=pl.ANY)
@@ -289,9 +319,12 @@
             pltpu.VMEM((2, units, cols), BF16),
             pltpu.VMEM((2, units, cols), BF16),
             pltpu.VMEM((n_ra, piece, cols), F32),
-            pltpu.VMEM((2, n_ra, piece, 2 * half), BF16),
-            pltpu.VMEM((2, 2, piece, 2 * half), BF16),
-            pltpu.VMEM((2, n_ra, piece, 2 * half), BF16),
+            pltpu.VMEM((2, n_ra, piece, 2 * units), BF16),
+            pltpu.VMEM((2, 2, piece, 2 * units), BF16),
+            pltpu.VMEM((2, n_ra, piece, 2 * units), BF16),
+            pltpu.VMEM((2, n_ra, 1, LANES), F32),
+            pltpu.VMEM((2, 2, 1, LANES), F32),
+            pltpu.VMEM((2, n_ra, 1, LANES), F32),
             pltpu.VMEM((2, piece, units), BF16),
             pltpu.VMEM((2, n_ra, piece, units), BF16),
             *(pltpu.VMEM((k, n_cb, rows // k, cols), BF16) for k in GROUPS),
@@ -300,7 +333,7 @@
             pltpu.SemaphoreType.REGULAR,
             pltpu.SemaphoreType.REGULAR,
             dma((9,)),
-            dma((2,)), dma((2, 5)),
+            dma((2,)), dma((2, 5)), dma((2,)), dma((2, 5)),
             dma((2,)), dma((2, max(GROUPS))),
             dma((2, max(GROUPS))), dma((2, max(GROUPS))),
         ],

time: 82.8 us -> 81.2 us (0.981)
  Pallas kernels: 82.1 us -> 80.5 us
    pallas_call x1, Pallas kernels: 82.1 us -> 80.5 us  [per_device(): pl.pallas_call(functools.partial(fused, n_ra, n_cb), out_shape=pltpu.VMEM...]
where the time goes in v6:
time: 81.2 us
  Pallas kernels  80.5 us (99%)
    pallas_call x1, Pallas kernels, per_device(): pl.pallas_call(functools.partial(fused, n_ra, n_cb), out_shape=pltpu.VMEM...  80.5 us

profile of v6, /device:TPU:33, one launch (start us, length us, event | category | flops | bytes accessed | tf_op | source)
XLA Modules:
  0.0 81.2 jit_solution(1555391304844488361)
XLA Ops:
  0.0 80.5 %shard_map.91 = bf16[16,8,128]{2,1,0:T(8,128)(2,1)S(1)} custom-call(bf16[128,128]{1,0:T(8,128)(2,1)} %tokens.1, bf16[1,128]{1,0:T(2,128)(2,1)} %bitcast.12, bf16[704,128]{1,0:T(8,128)(2,1)} %bitcast.8, bf16[704,128]{1,0:T(8,128)(2,1)} %bitcast.9, bf16[704,128]{1,0:T(8,128)(2,1)} %down1.1, bf16[1,128]{1,0:T(2,128)(2,1)} %bitcast.13, ...), custom_call_target="tpu_custom_call" | custom-call | tf_op jit(solution)/shard_map/pallas_call | solution.py:310
  80.5 0.6 copy.11

commit v7 on v6

--- a/solution.py
+++ b/solution.py
@@ -114,7 +114,7 @@
             sq_out[s, place] = jnp.sum(jnp.where(diagonal, sq[cut], 0.0), axis=0, keepdims=True)
 
     def batch(o):
-        return 0 if o in ahead else 1 if o in behind else 2 if o == hop else 3 if o == n_ra - hop else 4
+        return 0 if o in ahead else 1 if o in behind else 2 if o in relays else 3
 
     def all_of(ref, send_sem, recv_sem):
         return pltpu.make_async_remote_copy(
@@ -162,13 +162,13 @@
         group = [seen in g for g in all_groups[s]].index(True)
         return pltpu.make_async_remote_copy(
             src_ref=ag_out.at[s], dst_ref=ag_in.at[s, ra], send_sem=ag_send.at[s],
-            recv_sem=ag_recv.at[s, group], device_id={"ra": at(o)}, device_id_type=MESH)
+            recv_sem=ag_recv.at[s * GROUPS[0] + group], device_id={"ra": at(o)}, device_id_type=MESH)
 
     def gathered(s, count, recv_sem):
         return all_of(ag_in.at[s, pl.ds(0, count)], ag_send.at[s], recv_sem)
 
     def summed(s, g):
-        return all_of(ar_ins[s].at[g, pl.ds(0, n_cb - 1)], ar_send.at[s, g], ar_recv.at[s, g])
+        return all_of(ar_ins[s].at[g, pl.ds(0, n_cb - 1)], ar_send.at[s], ar_recv.at[s * GROUPS[0] + g])
 
     rs = [scatter(s) for s in range(2)]
     free = [o for o in far_first(n_ra) if o not in relays]
@@ -222,9 +222,9 @@
         for o in direct:
             total = total + rs_in[s, o].astype(F32)
             total_sq = total_sq + sq_in[s, o]
+        with scope(f"scatter_wait{s}_relays"):
+            arrived(s, len(relays), batch(hop))
         for o in relays:
-            with scope(f"scatter_wait{s}_{o}"):
-                arrived(s, 1, batch(o))
             total = total + rs_in[s, o].astype(F32)
             total_sq = total_sq + sq_in[s, o]
         sumsq = jnp.sum(jnp.where(diagonal, total_sq, 0.0), axis=1, keepdims=True)
@@ -256,13 +256,13 @@
         def down(g):
             with scope(f"gather_wait{s}_{g}"):
                 count = sum(o != 0 for o in groups[g])
-                gathered(s, count, ag_recv.at[s, g]).wait_recv()
+                gathered(s, count, ag_recv.at[s * GROUPS[0] + g]).wait_recv()
             h = jnp.concatenate([ag_in[s, at(o)].astype(F32) for o in groups[g]], axis=0).astype(BF16)
             ar_in[g, cb] = jnp.dot(h, down_v[s], preferred_element_type=F32).astype(BF16)
             for o in far_first(n_cb):
                 pltpu.make_async_remote_copy(
-                    src_ref=ar_in.at[g, cb], dst_ref=ar_in.at[g, cb], send_sem=ar_send.at[s, g],
-                    recv_sem=ar_recv.at[s, g], device_id={"cb": lax.rem(cb + o, n_cb)}, device_id_type=MESH).start()
+                    src_ref=ar_in.at[g, cb], dst_ref=ar_in.at[g, cb], send_sem=ar_send.at[s],
+                    recv_sem=ar_recv.at[s * GROUPS[0] + g], device_id={"cb": lax.rem(cb + o, n_cb)}, device_id_type=MESH).start()
 
         def finish(g):
             with scope(f"cb_wait{s}_{g}"):
@@ -292,11 +292,10 @@
                     pl.semaphore_wait(all_in, 1)
         for g in range(len(groups)):
             down(g)
-        gathered(s, n_ra - 1, ag_recv.at[s, 0]).wait_send()
+        gathered(s, n_ra - 1, ag_recv.at[s * GROUPS[0]]).wait_send()
         for g in range(len(groups)):
             finish(g)
-        for g in range(len(groups)):
-            summed(s, g).wait_send()
+        all_of(ar_in.at[pl.ds(0, len(groups)), pl.ds(0, n_cb - 1)], ar_send.at[s], ar_recv.at[0]).wait_send()
 
 
 def per_device(tokens, first_gain, first_gate, first_up, first_down,
@@ -333,9 +332,9 @@
             pltpu.SemaphoreType.REGULAR,
             pltpu.SemaphoreType.REGULAR,
             dma((9,)),
-            dma((2,)), dma((2, 5)), dma((2,)), dma((2, 5)),
-            dma((2,)), dma((2, max(GROUPS))),
-            dma((2, max(GROUPS))), dma((2, max(GROUPS))),
+            dma((2,)), dma((2, 4)), dma((2,)), dma((2, 4)),
+            dma((2,)), dma((sum(GROUPS),)),
+            dma((2,)), dma((sum(GROUPS),)),
         ],
         compiler_params=pltpu.CompilerParams(collective_id=0, has_side_effects=True),
     )(tokens, first_gain.reshape(1, -1), first_gate.T, first_up.T, first_down,

time: 81.2 us -> 81 us (level)
  no operation moved by 1% of the time
where the time goes in v7:
time: 81 us; the launch traced here: 80.9 us
  Pallas kernels  80.3 us (99%)
    pallas_call x1, Pallas kernels, per_device(): pl.pallas_call(functools.partial(fused, n_ra, n_cb), out_shape=pltpu.VMEM...  80.3 us

profile of v7, /device:TPU:33, one launch (start us, length us, event | category | flops | bytes accessed | tf_op | source)
XLA Modules:
  0.0 80.9 jit_solution(16032509153798574229)
XLA Ops:
  0.0 80.3 %shard_map.91 = bf16[16,8,128]{2,1,0:T(8,128)(2,1)S(1)} custom-call(bf16[128,128]{1,0:T(8,128)(2,1)} %tokens.1, bf16[1,128]{1,0:T(2,128)(2,1)} %bitcast.12, bf16[704,128]{1,0:T(8,128)(2,1)} %bitcast.8, bf16[704,128]{1,0:T(8,128)(2,1)} %bitcast.9, bf16[704,128]{1,0:T(8,128)(2,1)} %down1.1, bf16[1,128]{1,0:T(2,128)(2,1)} %bitcast.13, ...), custom_call_target="tpu_custom_call" | custom-call | tf_op jit(solution)/shard_map/pallas_call | solution.py:309
  80.3 0.6 copy.11
